TPU v7x, 32 devices: a whole 2x2x4 slice. The times are simulated.
32 devices in a mesh: ep: 8 (over z, y), tp: 4 (over x, core).
Axes of the slice: x: 2, y: 2, z: 4, core: 2. Of those that a mesh axis runs over, the one named last changes fastest.
Arguments:
- residual_in: bfloat16 [16, 2048], P('ep'), may hold values from -6 to 6
- gla_state: float32 [16, 4, 256, 512], P('ep', 'tp'), may hold values from -6 to 6
- norm_gain: bfloat16 [2048], replicated, may hold values from 0.099609375 to 1.8984375
- w_query: bfloat16 [2048, 1024], P('ep', 'tp'), may hold values from -0.125 to 0.125
- w_key: bfloat16 [2048, 1024], P('ep', 'tp'), may hold values from -0.125 to 0.125
- w_value: bfloat16 [2048, 2048], P('ep', 'tp'), may hold values from -0.125 to 0.125
- w_decay: bfloat16 [2048, 1024], P('ep', 'tp'), may hold values from -0.5 to 0.5
- decay_bias: float32 [1024], P('tp'), may hold values from -40 to 8
- head_gain: bfloat16 [512], replicated, may hold values from 0.099609375 to 1.8984375
- w_output: bfloat16 [2048, 2048], P('tp', 'ep'), may hold values from -0.125 to 0.125
- ffn_gain: bfloat16 [2048], replicated, may hold values from 0.099609375 to 1.8984375
- router_group: bfloat16 [2048, 4], replicated, may hold values from -0.125 to 0.125
- router_expert: bfloat16 [8, 2048], replicated, may hold values from -0.125 to 0.125
- expert_ids: int32 [16, 2], replicated, may hold values from 0 to 7, all different within a row; in each aligned block of 16 rows (0 to 15, 16 to 31, ...) at most 16 rows name the same one
- w_gate: bfloat16 [8, 2048, 512], P('ep', None, 'tp'), may hold values from -0.125 to 0.125
- w_up: bfloat16 [8, 2048, 512], P('ep', None, 'tp'), may hold values from -0.125 to 0.125
- w_down: bfloat16 [8, 512, 2048], P('ep', 'tp'), may hold values from -0.75 to 0.75
Outputs:
- layer_out: bfloat16 [16, 2048], P('ep')
- new_state: float32 [16, 4, 256, 512], P('ep', 'tp')
Inputs may be any that keep to these rules, and one draw needn't show every extreme that they name: `expert_ids`: each row names 2 different experts; no expert is named by more than 16 rows of the whole batch, a bound that some block reaches.
All inputs are finite; a program needn't handle non-finite values.
Results may differ from a plain program's by a relative error of at most 0.023.
Values may be sent and summed in bfloat16 or wider, within the bound.
A program may use at most 64 MiB of HBM per device.

v0:
```python
import jax
import jax.numpy as jnp
from jax import lax
from jax.sharding import PartitionSpec as P

CAP = 16
EPSILON = 1e-06
GATE_SCALE = 16.0


def rms_scale(values, gain_vec):
    floats = values.astype(jnp.float32)
    return (
        floats
        * lax.rsqrt(jnp.mean(floats * floats, axis=-1, keepdims=True) + EPSILON)
        * gain_vec.astype(jnp.float32)
    )


def finish_part(hidden_res, moe_part, tp_index):
    part_cols = moe_part.shape[1]
    own_cols = lax.dynamic_slice_in_dim(hidden_res, tp_index * part_cols, part_cols, 1)
    return (own_cols.astype(jnp.float32) + moe_part).astype(jnp.bfloat16)


def on_device(
    residual_in,
    gla_state,
    norm_gain,
    w_query,
    w_key,
    w_value,
    w_decay,
    decay_bias,
    head_gain,
    w_output,
    ffn_gain,
    router_group,
    router_expert,
    expert_ids,
    w_gate,
    w_up,
    w_down,
):
    seq_rows = residual_in.shape[0]
    key_width = w_query.shape[1]
    value_width = w_value.shape[1]
    normed = rms_scale(residual_in, norm_gain).astype(jnp.bfloat16)
    columns = lax.all_to_all(normed, "ep", split_axis=1, concat_axis=0, tiled=True)
    projected = lax.psum_scatter(
        jnp.concatenate(
            [
                jnp.dot(columns, w_query, preferred_element_type=jnp.float32),
                jnp.dot(columns, w_key, preferred_element_type=jnp.float32),
                jnp.dot(columns, w_value, preferred_element_type=jnp.float32),
                jnp.dot(columns, w_decay, preferred_element_type=jnp.float32),
            ],
            axis=1,
        ),
        "ep",
        scatter_dimension=0,
        tiled=True,
    )
    query_rows = projected[:, :key_width].astype(jnp.bfloat16)
    key_rows = projected[:, key_width : 2 * key_width].astype(jnp.bfloat16)
    value_rows = projected[:, 2 * key_width : 2 * key_width + value_width].astype(jnp.bfloat16)
    decay_pre = projected[:, 2 * key_width + value_width :]
    log_decay = jax.nn.log_sigmoid(decay_pre + decay_bias) / GATE_SCALE
    query_float = lax.optimization_barrier(query_rows).astype(jnp.float32) * key_width ** (-0.5)
    key_float = lax.optimization_barrier(key_rows).astype(jnp.float32)
    value_float = lax.optimization_barrier(value_rows).astype(jnp.float32)
    old_state = gla_state[:, 0]
    new_state = (
        jnp.exp(log_decay)[:, :, None] * old_state + key_float[:, :, None] * value_float[:, None, :]
    )
    read_out = jnp.einsum("tk,tkv->tv", query_float, new_state, precision=lax.Precision.HIGHEST)
    gated_heads = rms_scale(read_out, head_gain).astype(jnp.bfloat16)
    partial_out = jnp.dot(
        lax.all_gather(gated_heads, "ep", axis=0, tiled=True),
        w_output,
        preferred_element_type=jnp.float32,
    ).astype(jnp.bfloat16)
    returned = lax.all_to_all(partial_out, "ep", split_axis=0, concat_axis=1, tiled=True)
    attention = lax.psum(returned.astype(jnp.float32).astype(jnp.bfloat16), "tp").astype(
        jnp.float32
    )
    hidden_res = (residual_in.astype(jnp.float32) + attention).astype(jnp.bfloat16)
    moe_in = rms_scale(hidden_res, ffn_gain).astype(jnp.bfloat16)
    expert = lax.axis_index("ep")
    is_named = jnp.any(expert_ids == expert, axis=1)
    slot_of = jnp.cumsum(is_named.astype(jnp.int32)) - 1
    slot_index = jnp.arange(CAP, dtype=jnp.int32)
    select_int = (is_named[None, :] & (slot_of[None, :] == slot_index[:, None])).astype(jnp.int32)
    select_bf = select_int.astype(jnp.bfloat16)
    slot_rows = jnp.dot(
        select_bf,
        lax.all_gather(moe_in, "ep", axis=0, tiled=True),
        preferred_element_type=jnp.float32,
    ).astype(jnp.bfloat16)
    slot_ids = jnp.sum(select_int[:, :, None] * expert_ids[None, :, :], axis=1)
    rival_ids = jnp.where(slot_ids[:, 0] == expert, slot_ids[:, 1], slot_ids[:, 0])
    group_logits = jnp.dot(slot_rows, router_group, preferred_element_type=jnp.float32)
    per_group = router_expert.shape[0] // router_group.shape[1]
    own_group = jnp.arange(router_group.shape[1], dtype=jnp.int32) == expert // per_group
    group_logit = jnp.sum(
        jnp.where(own_group[None, :], group_logits, jnp.zeros_like(group_logits)), axis=1
    )
    group_share = 1.0 / jnp.sum(jnp.exp(group_logits - group_logit[:, None]), axis=1)
    chosen = jnp.dot(slot_rows, router_expert[expert], preferred_element_type=jnp.float32)
    rival_logit = jnp.einsum(
        "cd,cd->c", slot_rows, router_expert[rival_ids], preferred_element_type=jnp.float32
    )
    slot_weight = group_share * jax.nn.sigmoid(chosen - rival_logit)
    gate_out = jnp.dot(slot_rows, w_gate[0], preferred_element_type=jnp.float32)
    up_out = jnp.dot(slot_rows, w_up[0], preferred_element_type=jnp.float32)
    hidden = (jax.nn.silu(gate_out) * up_out).astype(jnp.bfloat16)
    output = jnp.dot(hidden, w_down[0], preferred_element_type=jnp.float32)
    select_float = select_int.astype(jnp.float32)
    width_piece = lax.psum_scatter(
        output.astype(jnp.bfloat16), "tp", scatter_dimension=1, tiled=True
    ).astype(jnp.float32)
    weighted_piece = width_piece * slot_weight[:, None]
    piece_cols = weighted_piece.shape[1]
    outgoing = jnp.dot(select_float.T, weighted_piece, precision=lax.Precision.HIGHEST)
    owners = outgoing.shape[0] // seq_rows
    outgoing = outgoing.reshape(owners, seq_rows, piece_cols)
    arrived = lax.all_to_all(
        outgoing.astype(jnp.bfloat16), "ep", split_axis=0, concat_axis=0, tiled=True
    ).astype(outgoing.dtype)
    moe_piece = jnp.sum(arrived, axis=0)
    layer_piece = finish_part(hidden_res, moe_piece, lax.axis_index("tp"))
    layer_out = lax.all_gather(layer_piece, "tp", axis=1, tiled=True)
    return (layer_out, new_state[:, None])


def solution(mesh):
    placed = (
        P("ep", None),
        P("ep", "tp", None, None),
        P(),
        P("ep", "tp"),
        P("ep", "tp"),
        P("ep", "tp"),
        P("ep", "tp"),
        P("tp"),
        P(),
        P("tp", "ep"),
        P(),
        P(),
        P(),
        P(),
        P("ep", None, "tp"),
        P("ep", None, "tp"),
        P("ep", "tp", None),
    )
    return jax.shard_map(
        on_device,
        mesh=mesh,
        in_specs=placed,
        out_specs=(P("ep", None), P("ep", "tp", None, None)),
        check_vma=False,
    )
```

profile of v0, /device:TPU:0, one launch (start us, length us, event | category | flops | bytes accessed | tf_op | source)
XLA Modules:
  0.0 217.5 jit_solution(11208701178793737976)
XLA Ops:
  7.2 0.0 copy-start
  7.2 0.0 copy-start.12
  7.2 0.0 copy-start.8
  7.2 0.0 copy-start.6
  7.2 0.0 copy-start.2
  7.2 0.9 fusion.25
  8.2 0.0 copy-done.8
  8.2 1.4 fusion.27
  9.6 7.3 %all-to-all-start = ((bf16[2,8,256]{2,0,1:T(2,128)(2,1)}), bf16[2,8,256]{2,0,1:T(2,128)(2,1)S(1)}, u32[]{:S(2)}, u32[]{:S(2)}) async-start(bf16[2,8,256]{2,0,1:T(2,128)(2,1)} %bitcast), calls=%async_computation | async-start | bytes 16384 | tf_op jit(solution)/shard_map/all_to_all | solution.py:49
  16.9 0.0 all-reduce.3.cloned.1.call-start
  16.9 0.7 compare_reduce_fusion
  17.6 0.1 copy.30
  17.8 0.1 add_reduce_fusion
  17.9 0.8 multiply_reduce_fusion
  18.7 0.7 convert_element_type.109
  19.4 0.6 dynamic-slice
  20.6 2.8 %all-to-all-done = bf16[2,8,256]{2,0,1:T(2,128)(2,1)S(1)} async-done(((bf16[2,8,256]{2,0,1:T(2,128)(2,1)}), bf16[2,8,256]{2,0,1:T(2,128)(2,1)S(1)}, u32[]{:S(2)}, u32[]{:S(2)}) %all-to-all-start) | async-done | bytes 8224 | tf_op jit(solution)/shard_map/all_to_all | solution.py:49
  23.4 0.0 copy-done.6
  23.4 0.1 fusion.66
  23.6 1.1 fusion.64
  24.6 1.1 fusion.63
  25.7 1.1 fusion.65
  26.8 0.7 pad_maximum_fusion
  27.4 0.0 all-reduce.3.cloned.1.call-update
  27.5 68.3 %all-reduce.3.cloned.1.call-done = f32[16,1280]{1,0:T(8,128)} async-done(((f32[16,1280]{1,0:T(8,128)}), f32[16,1280]{1,0:T(8,128)}) %all-reduce.3.cloned.1.call-update) | async-done | bytes 81936
  95.7 0.8 dynamic-slice_convert_fusion
  96.6 0.0 copy-start.10
  96.6 0.7 copy-done.10
  97.2 0.8 fusion.54
  98.0 0.0 copy-start.5
  98.1 0.8 fusion.8
  98.8 0.1 fusion.44
  99.0 0.1 fusion.57
  99.0 26.1 %all-gather = bf16[8,2,512]{2,1,0:T(2,128)(2,1)S(1)} all-gather(bf16[1,2,512]{2,1,0:T(2,128)(2,1)S(1)} %fusion.57), channel_id=1, replica_groups=mesh['ep'=8,'tp'=4] {'ep'}, dimensions={0}, use_global_device_ids=true | all-gather | bytes 18432 | tf_op jit(solution)/shard_map/all_gather | solution.py:79
  125.2 0.1 convolution_convert_fusion.3
  125.3 0.6 all_to_all.35
  126.0 3.3 %all-to-all-start.1 = ((bf16[8,2,256]{2,1,0:T(2,128)(2,1)}), bf16[8,2,256]{2,1,0:T(2,128)(2,1)S(1)}, u32[]{:S(2)}, u32[]{:S(2)}) async-start(bf16[8,2,256]{2,1,0:T(2,128)(2,1)} %all_to_all.35), calls=%async_computation.1 | async-start | bytes 16384 | tf_op jit(solution)/shard_map/all_to_all | solution.py:83
  129.3 0.0 reduce-scatter.2.cloned.1.call-start
  129.4 0.0 copy-start.9
  129.4 0.7 copy-done.9
  130.1 0.6 gather_fusion
  130.7 5.1 %all-to-all-done.1 = bf16[8,2,256]{2,1,0:T(2,128)(2,1)S(1)} async-done(((bf16[8,2,256]{2,1,0:T(2,128)(2,1)}), bf16[8,2,256]{2,1,0:T(2,128)(2,1)S(1)}, u32[]{:S(2)}, u32[]{:S(2)}) %all-to-all-start.1) | async-done | bytes 8224 | tf_op jit(solution)/shard_map/all_to_all | solution.py:83
  135.8 5.9 %psum.7 = bf16[2,2048]{1,0:T(2,128)(2,1)S(1)} all-reduce(bf16[2,2048]{1,0:T(2,128)(2,1)S(1)} %bitcast.76), channel_id=1, replica_groups=mesh['ep'=8,'tp'=4] {'tp'}, use_global_device_ids=true, to_apply=%region_3.4 | all-reduce | flops 4096 | bytes 16384 | tf_op jit(solution)/shard_map/psum | solution.py:84
  141.6 0.0 copy-done.7
  141.6 0.0 copy-start.3
  141.7 0.1 fusion.22
  141.8 0.1 fusion.38
  141.9 30.5 %all-gather.1 = bf16[8,2,2048]{2,1,0:T(2,128)(2,1)S(1)} all-gather(bf16[1,2,2048]{2,1,0:T(2,128)(2,1)S(1)} %fusion.38), channel_id=1, replica_groups=mesh['ep'=8,'tp'=4] {'ep'}, dimensions={0}, use_global_device_ids=true | all-gather | bytes 73728 | tf_op jit(solution)/shard_map/all_gather | solution.py:97
  172.5 0.2 fusion.19
  172.7 0.2 fusion.14
  172.9 0.0 copy-done.3
  172.9 1.0 convolution_convert_fusion
  173.9 0.0 reduce-scatter.2.cloned.1.call-update
  173.9 0.7 copy-done.11
  174.6 0.1 select_reduce_fusion
  174.8 0.1 fusion.6
  174.9 16.2 %reduce-scatter.2.cloned.1.call-done = bf16[16,512]{1,0:T(8,128)(2,1)} async-done(((bf16[16,2048]{1,0:T(8,128)(2,1)}), bf16[16,512]{1,0:T(8,128)(2,1)}) %reduce-scatter.2.cloned.1.call-update) | async-done | bytes 16400 | tf_op jit(solution)/shard_map/reduce_scatter | solution.py:119
  191.2 0.9 convolution_convert_fusion.2
  192.1 0.6 convert_element_type.128
  192.7 5.5 %all-to-all-start.2 = ((bf16[8,2,512]{2,1,0:T(2,128)(2,1)}), bf16[8,2,512]{2,1,0:T(2,128)(2,1)S(1)}, u32[]{:S(2)}, u32[]{:S(2)}) async-start(bf16[8,2,512]{2,1,0:T(2,128)(2,1)} %convert_element_type.128), calls=%async_computation.3 | async-start | bytes 32768 | tf_op jit(solution)/shard_map/all_to_all | solution.py:127
  198.2 1.2 multiply_add_fusion
  199.4 5.4 %all-to-all-done.2 = bf16[8,2,512]{2,1,0:T(2,128)(2,1)S(1)} async-done(((bf16[8,2,512]{2,1,0:T(2,128)(2,1)}), bf16[8,2,512]{2,1,0:T(2,128)(2,1)S(1)}, u32[]{:S(2)}, u32[]{:S(2)}) %all-to-all-start.2) | async-done | bytes 16416 | tf_op jit(solution)/shard_map/all_to_all | solution.py:127
  204.9 5.2 %all_gather.11 = bf16[2,2048]{1,0:T(2,128)(2,1)S(1)} all-gather(bf16[2,512]{1,0:T(2,128)(2,1)S(1)} %add_convert_fusion), channel_id=1, replica_groups=mesh['ep'=8,'tp'=4] {'tp'}, dimensions={1}, use_global_device_ids=true | all-gather | bytes 10240 | tf_op jit(solution)/shard_map/all_gather | solution.py:132
  210.1 0.6 copy.46
  (32 shorter events, 0.3 us)
Async XLA Ops:
  7.2 165.7 %copy-start = (bf16[1,128,2048]{2,1,0:T(8,128)(2,1)S(1)}, bf16[1,128,2048]{2,1,0:T(8,128)(2,1)}, u32[]{:S(2)}) copy-start(bf16[1,128,2048]{2,1,0:T(8,128)(2,1)} %param.33) | copy-start | bytes 1572868
  7.2 12.2 %copy-start.12 = (u32[32]{0:T(128)S(1)}, u32[32]{0:T(128)}, u32[]{:S(2)}) copy-start(u32[32]{0:T(128)} %constant.70) | copy-start | bytes 388
  7.2 1.0 copy-start.8
  7.2 16.2 %copy-start.6 = (bf16[256,256]{1,0:T(8,128)(2,1)S(1)}, bf16[256,256]{1,0:T(8,128)(2,1)}, u32[]{:S(2)}) copy-start(bf16[256,256]{1,0:T(8,128)(2,1)} %param.23) | copy-start | bytes 393220
  7.2 90.8 %copy-start.2 = (f32[2,1,256,512]{3,2,1,0:T(8,128)S(1)}, f32[2,1,256,512]{3,2,1,0:T(8,128)}, u32[]{:S(2)}) copy-start(f32[2,1,256,512]{3,2,1,0:T(8,128)} %param.18) | copy-start | bytes 3145732
  9.6 13.8 %all-to-all-start = ((bf16[2,8,256]{2,0,1:T(2,128)(2,1)}), bf16[2,8,256]{2,0,1:T(2,128)(2,1)S(1)}, u32[]{:S(2)}, u32[]{:S(2)}) async-start(bf16[2,8,256]{2,0,1:T(2,128)(2,1)} %bitcast), calls=%async_computation | async-start | bytes 16384 | tf_op jit(solution)/shard_map/all_to_all | solution.py:49
  16.9 78.8 %all-reduce.3.cloned.1.call-start = ((), (), s32[]{:S(2)}) async-start(), calls=%async_computation.5 | async-start | bytes 163840
  96.6 0.7 copy-start.10
  98.0 27.1 %copy-start.5 = (bf16[512,256]{1,0:T(8,128)(2,1)S(1)}, bf16[512,256]{1,0:T(8,128)(2,1)}, u32[]{:S(2)}) copy-start(bf16[512,256]{1,0:T(8,128)(2,1)} %param.26) | copy-start | bytes 786436
  125.3 4.7 %copy-start.1 = (bf16[8,2048]{1,0:T(8,128)(2,1)S(1)}, bf16[8,2048]{1,0:T(8,128)(2,1)}, u32[]{:S(2)}) copy-start(bf16[8,2048]{1,0:T(8,128)(2,1)} %param.29) | copy-start | bytes 98308
  126.0 9.8 %all-to-all-start.1 = ((bf16[8,2,256]{2,1,0:T(2,128)(2,1)}), bf16[8,2,256]{2,1,0:T(2,128)(2,1)S(1)}, u32[]{:S(2)}, u32[]{:S(2)}) async-start(bf16[8,2,256]{2,1,0:T(2,128)(2,1)} %all_to_all.35), calls=%async_computation.1 | async-start | bytes 16384 | tf_op jit(solution)/shard_map/all_to_all | solution.py:83
  129.3 61.9 %reduce-scatter.2.cloned.1.call-start = ((), (), s32[]{:S(2)}) async-start(), calls=%async_computation.4 | async-start | bytes 81920 | tf_op jit(solution)/shard_map/reduce_scatter | solution.py:119
  129.4 0.7 copy-start.9
  130.1 42.6 %copy-start.4 = (bf16[1,2048,128]{2,1,0:T(8,128)(2,1)S(1)}, bf16[1,2048,128]{2,1,0:T(8,128)(2,1)}, u32[]{:S(2)}) copy-start(bf16[1,2048,128]{2,1,0:T(8,128)(2,1)} %param.31) | copy-start | bytes 1572868
  135.8 5.9 %copy-start.7 = (bf16[2,2048]{1,0:T(2,128)(2,1)S(1)}, bf16[2,2048]{1,0:T(2,128)(2,1)}, u32[]{:S(2)}) copy-start(bf16[2,2048]{1,0:T(2,128)(2,1)} %param.17) | copy-start | bytes 24580
  141.6 31.3 %copy-start.3 = (bf16[1,2048,128]{2,1,0:T(8,128)(2,1)S(1)}, bf16[1,2048,128]{2,1,0:T(8,128)(2,1)}, u32[]{:S(2)}) copy-start(bf16[1,2048,128]{2,1,0:T(8,128)(2,1)} %param.32) | copy-start | bytes 1572868
  173.9 0.7 copy-start.11
  192.7 12.1 %all-to-all-start.2 = ((bf16[8,2,512]{2,1,0:T(2,128)(2,1)}), bf16[8,2,512]{2,1,0:T(2,128)(2,1)S(1)}, u32[]{:S(2)}, u32[]{:S(2)}) async-start(bf16[8,2,512]{2,1,0:T(2,128)(2,1)} %convert_element_type.128), calls=%async_computation.3 | async-start | bytes 32768 | tf_op jit(solution)/shard_map/all_to_all | solution.py:127
Sparse Core Ops, SparseCore 0:
  27.6 68.1 all-reduce.2
  174.0 17.0 reduce-scatter.1
where the time goes:
time: 218 us; the launch traced here: 217 us
  waiting for transfers between devices  97.8 us (45%)
  blocking collectives  67.7 us (31%)
  starting transfers between devices  16.2 us (7%)
  between operations  15 us (7%)
  other arithmetic  7.82 us (4%)
  matrix products  6.92 us (3%)
  local copies, waits for them, and re-layouts  6.05 us (3%)
    unnamed x3, waiting for transfers between devices  68.3 us
    all_gather x1, blocking collectives, on_device(): lax.all_gather(moe_in, 'ep', axis=0, tiled=True)  30.5 us
    all_gather x1, blocking collectives, on_device(): lax.all_gather(gated_heads, 'ep', axis=0, tiled=True)  26.1 us
    reduce_scatter x1, waiting for transfers between devices, on_device(): lax.psum_scatter(output.astype(jnp.bfloat16), 'tp', scatter_dimension=1,...  16.2 us
    all_to_all x1, starting transfers between devices, on_device(): lax.all_to_all(normed, 'ep', split_axis=1, concat_axis=0, tiled=True)  7.31 us
    psum x1, blocking collectives, on_device(): lax.psum(returned.astype(jnp.float32).astype(jnp.bfloat16), 'tp')  5.87 us
    all_to_all x1, starting transfers between devices, on_device(): lax.all_to_all(outgoing.astype(jnp.bfloat16), 'ep', split_axis=0, concat_...  5.52 us
    all_to_all x1, waiting for transfers between devices, on_device(): lax.all_to_all(outgoing.astype(jnp.bfloat16), 'ep', split_axis=0, concat_...  5.4 us
  transfers between devices with their start and end apart: 5, of which 5 were waited for; matrix products, arithmetic and copies ran while one was open for 2% of the time, Pallas kernels for 0%

commit v1 on v0

--- a/solution.py
+++ b/solution.py
@@ -76,7 +76,9 @@
     read_out = jnp.einsum("tk,tkv->tv", query_float, new_state, precision=lax.Precision.HIGHEST)
     gated_heads = rms_scale(read_out, head_gain).astype(jnp.bfloat16)
     partial_out = jnp.dot(
-        lax.all_gather(gated_heads, "ep", axis=0, tiled=True),
+        jnp.concatenate(
+            lax.all_to_all(jnp.stack([gated_heads] * lax.axis_size("ep")), "ep", 0, 0), axis=0
+        ),
         w_output,
         preferred_element_type=jnp.float32,
     ).astype(jnp.bfloat16)

time: 218 us -> 202 us (0.927)
  blocking collectives: 67.7 us -> 41.6 us
  starting transfers between devices: 16.2 us -> 20.5 us
  waiting for transfers between devices: 97.8 us -> 102 us
    all_gather x1 -> x0, blocking collectives: 26.1 us -> none  [on_device(): lax.all_gather(gated_heads, 'ep', axis=0, tiled=True)]
    all_to_all x0 -> x1, waiting for transfers between devices: none -> 6.56 us  [on_device(): lax.all_to_all(jnp.stack([gated_heads] * lax.axis_size('ep')), 'ep', 0, 0)]
    all_to_all x0 -> x1, starting transfers between devices: none -> 4.31 us  [on_device(): lax.all_to_all(jnp.stack([gated_heads] * lax.axis_size('ep')), 'ep', 0, 0)]
    unnamed x3, waiting for transfers between devices: 68.3 us -> 64.4 us
  transfers between devices with their start and end apart: 5 -> 6, of which waited for: 5 -> 6; matrix products, arithmetic and copies ran while one was open for 2% -> 3% of each run, Pallas kernels for 0% -> 0%
where the time goes in v1:
time: 202 us
  waiting for transfers between devices  102 us (50%)
  blocking collectives  41.6 us (21%)
  starting transfers between devices  20.5 us (10%)
  between operations  15 us (7%)
  other arithmetic  7.82 us (4%)
  local copies, waits for them, and re-layouts  7.33 us (4%)
  matrix products  6.92 us (3%)
    unnamed x3, waiting for transfers between devices  64.4 us
    all_gather x1, blocking collectives, on_device(): lax.all_gather(moe_in, 'ep', axis=0, tiled=True)  30.5 us
    reduce_scatter x1, waiting for transfers between devices, on_device(): lax.psum_scatter(output.astype(jnp.bfloat16), 'tp', scatter_dimension=1,...  16.2 us
    all_to_all x1, starting transfers between devices, on_device(): lax.all_to_all(normed, 'ep', split_axis=1, concat_axis=0, tiled=True)  7.31 us
    all_to_all x1, waiting for transfers between devices, on_device(): lax.all_to_all(jnp.stack([gated_heads] * lax.axis_size('ep')), 'ep', 0, 0)  6.56 us
    psum x1, blocking collectives, on_device(): lax.psum(returned.astype(jnp.float32).astype(jnp.bfloat16), 'tp')  5.87 us
    all_to_all x1, starting transfers between devices, on_device(): lax.all_to_all(outgoing.astype(jnp.bfloat16), 'ep', split_axis=0, concat_...  5.52 us
    all_to_all x1, waiting for transfers between devices, on_device(): lax.all_to_all(outgoing.astype(jnp.bfloat16), 'ep', split_axis=0, concat_...  5.4 us
  transfers between devices with their start and end apart: 6, of which 6 were waited for; matrix products, arithmetic and copies ran while one was open for 3% of the time, Pallas kernels for 0%

profile of v1, /device:TPU:0, one launch (start us, length us, event | category | flops | bytes accessed | tf_op | source)
XLA Modules:
  0.0 201.6 jit_solution(13043827727415094204)
XLA Ops:
  7.2 0.0 copy-start
  7.2 0.0 copy-start.8
  7.2 0.9 fusion.25
  8.2 0.0 copy-done.8
  8.2 1.4 fusion.27
  9.6 7.3 %all-to-all-start = ((bf16[2,8,256]{2,0,1:T(2,128)(2,1)}), bf16[2,8,256]{2,0,1:T(2,128)(2,1)S(1)}, u32[]{:S(2)}, u32[]{:S(2)}) async-start(bf16[2,8,256]{2,0,1:T(2,128)(2,1)} %bitcast), calls=%async_computation | async-start | bytes 16384 | tf_op jit(solution)/shard_map/all_to_all | solution.py:49
  16.9 0.0 all-reduce.3.cloned.1.call-start
  16.9 0.7 compare_reduce_fusion
  17.6 0.1 copy.30
  17.8 0.1 add_reduce_fusion
  17.9 0.8 multiply_reduce_fusion
  18.7 4.7 %all-to-all-done = bf16[2,8,256]{2,0,1:T(2,128)(2,1)S(1)} async-done(((bf16[2,8,256]{2,0,1:T(2,128)(2,1)}), bf16[2,8,256]{2,0,1:T(2,128)(2,1)S(1)}, u32[]{:S(2)}, u32[]{:S(2)}) %all-to-all-start) | async-done | bytes 8224 | tf_op jit(solution)/shard_map/all_to_all | solution.py:49
  23.4 0.1 fusion.65
  23.5 1.1 fusion.63
  24.6 1.1 fusion.62
  25.7 1.1 fusion.64
  26.8 0.7 pad_maximum_fusion
  27.4 0.0 all-reduce.3.cloned.1.call-update
  27.5 0.7 convert_element_type.109
  28.1 0.7 copy-done.12
  28.8 0.6 dynamic-slice
  30.0 64.4 %all-reduce.3.cloned.1.call-done = f32[16,1280]{1,0:T(8,128)} async-done(((f32[16,1280]{1,0:T(8,128)}), f32[16,1280]{1,0:T(8,128)}) %all-reduce.3.cloned.1.call-update) | async-done | bytes 81936
  94.4 0.8 dynamic-slice_convert_fusion
  95.2 0.0 copy-start.10
  95.2 0.7 copy-done.10
  95.9 0.8 fusion.54
  96.7 0.0 copy-start.5
  96.7 0.8 fusion.8
  97.5 0.1 fusion.44
  97.6 0.1 fusion.46
  97.7 0.6 stack.2
  98.3 4.3 %all-to-all-start.1 = ((bf16[8,2,512]{2,1,0:T(2,128)(2,1)}), bf16[8,2,512]{2,1,0:T(2,128)(2,1)S(1)}, u32[]{:S(2)}, u32[]{:S(2)}) async-start(bf16[8,2,512]{2,1,0:T(2,128)(2,1)} %stack.2), calls=%async_computation.1 | async-start | bytes 32768 | tf_op jit(solution)/shard_map/all_to_all | solution.py:80
  102.7 6.6 %all-to-all-done.1 = bf16[8,2,512]{2,1,0:T(2,128)(2,1)S(1)} async-done(((bf16[8,2,512]{2,1,0:T(2,128)(2,1)}), bf16[8,2,512]{2,1,0:T(2,128)(2,1)S(1)}, u32[]{:S(2)}, u32[]{:S(2)}) %all-to-all-start.1) | async-done | bytes 16416 | tf_op jit(solution)/shard_map/all_to_all | solution.py:80
  109.2 0.1 convolution_convert_fusion.3
  109.4 0.6 all_to_all.39
  110.0 3.3 %all-to-all-start.2 = ((bf16[8,2,256]{2,1,0:T(2,128)(2,1)}), bf16[8,2,256]{2,1,0:T(2,128)(2,1)S(1)}, u32[]{:S(2)}, u32[]{:S(2)}) async-start(bf16[8,2,256]{2,1,0:T(2,128)(2,1)} %all_to_all.39), calls=%async_computation.2 | async-start | bytes 16384 | tf_op jit(solution)/shard_map/all_to_all | solution.py:85
  113.4 0.0 reduce-scatter.2.cloned.1.call-start
  113.4 0.0 copy-start.9
  113.4 0.7 copy-done.9
  114.1 0.0 copy-done.1
  114.1 0.6 gather_fusion
  114.7 5.1 %all-to-all-done.2 = bf16[8,2,256]{2,1,0:T(2,128)(2,1)S(1)} async-done(((bf16[8,2,256]{2,1,0:T(2,128)(2,1)}), bf16[8,2,256]{2,1,0:T(2,128)(2,1)S(1)}, u32[]{:S(2)}, u32[]{:S(2)}) %all-to-all-start.2) | async-done | bytes 8224 | tf_op jit(solution)/shard_map/all_to_all | solution.py:85
  119.8 5.9 %psum.7 = bf16[2,2048]{1,0:T(2,128)(2,1)S(1)} all-reduce(bf16[2,2048]{1,0:T(2,128)(2,1)S(1)} %bitcast.71), channel_id=1, replica_groups=mesh['ep'=8,'tp'=4] {'tp'}, use_global_device_ids=true, to_apply=%region_3.4 | all-reduce | flops 4096 | bytes 16384 | tf_op jit(solution)/shard_map/psum | solution.py:86
  125.7 0.0 copy-start.3
  125.7 0.1 fusion.22
  125.9 0.1 fusion.38
  125.9 30.5 %all-gather = bf16[8,2,2048]{2,1,0:T(2,128)(2,1)S(1)} all-gather(bf16[1,2,2048]{2,1,0:T(2,128)(2,1)S(1)} %fusion.38), channel_id=1, replica_groups=mesh['ep'=8,'tp'=4] {'ep'}, dimensions={0}, use_global_device_ids=true | all-gather | bytes 73728 | tf_op jit(solution)/shard_map/all_gather | solution.py:99
  156.5 0.3 fusion.19
  156.8 0.0 copy-done.4
  156.8 0.2 fusion.14
  157.0 0.0 copy-done.3
  157.0 1.0 convolution_convert_fusion
  158.0 0.0 reduce-scatter.2.cloned.1.call-update
  158.0 0.7 copy-done.11
  158.7 0.1 select_reduce_fusion
  158.9 0.1 fusion.6
  159.0 16.2 %reduce-scatter.2.cloned.1.call-done = bf16[16,512]{1,0:T(8,128)(2,1)} async-done(((bf16[16,2048]{1,0:T(8,128)(2,1)}), bf16[16,512]{1,0:T(8,128)(2,1)}) %reduce-scatter.2.cloned.1.call-update) | async-done | bytes 16400 | tf_op jit(solution)/shard_map/reduce_scatter | solution.py:121
  175.2 0.9 convolution_convert_fusion.2
  176.2 0.6 convert_element_type.128
  176.8 5.5 %all-to-all-start.3 = ((bf16[8,2,512]{2,1,0:T(2,128)(2,1)}), bf16[8,2,512]{2,1,0:T(2,128)(2,1)S(1)}, u32[]{:S(2)}, u32[]{:S(2)}) async-start(bf16[8,2,512]{2,1,0:T(2,128)(2,1)} %convert_element_type.128), calls=%async_computation.4 | async-start | bytes 32768 | tf_op jit(solution)/shard_map/all_to_all | solution.py:129
  182.3 1.2 multiply_add_fusion
  183.5 5.4 %all-to-all-done.3 = bf16[8,2,512]{2,1,0:T(2,128)(2,1)S(1)} async-done(((bf16[8,2,512]{2,1,0:T(2,128)(2,1)}), bf16[8,2,512]{2,1,0:T(2,128)(2,1)S(1)}, u32[]{:S(2)}, u32[]{:S(2)}) %all-to-all-start.3) | async-done | bytes 16416 | tf_op jit(solution)/shard_map/all_to_all | solution.py:129
  188.9 5.2 %all_gather.7 = bf16[2,2048]{1,0:T(2,128)(2,1)S(1)} all-gather(bf16[2,512]{1,0:T(2,128)(2,1)S(1)} %add_convert_fusion), channel_id=1, replica_groups=mesh['ep'=8,'tp'=4] {'tp'}, dimensions={1}, use_global_device_ids=true | all-gather | bytes 10240 | tf_op jit(solution)/shard_map/all_gather | solution.py:134
  194.1 0.6 copy.44
  (34 shorter events, 0.3 us)
Async XLA Ops:
  7.2 149.8 %copy-start = (bf16[1,128,2048]{2,1,0:T(8,128)(2,1)S(1)}, bf16[1,128,2048]{2,1,0:T(8,128)(2,1)}, u32[]{:S(2)}) copy-start(bf16[1,128,2048]{2,1,0:T(8,128)(2,1)} %param.33) | copy-start | bytes 1572868
  7.2 1.0 copy-start.8
  7.2 16.2 %copy-start.6 = (bf16[256,256]{1,0:T(8,128)(2,1)S(1)}, bf16[256,256]{1,0:T(8,128)(2,1)}, u32[]{:S(2)}) copy-start(bf16[256,256]{1,0:T(8,128)(2,1)} %param.23) | copy-start | bytes 393220
  7.2 89.5 %copy-start.2 = (f32[2,1,256,512]{3,2,1,0:T(8,128)S(1)}, f32[2,1,256,512]{3,2,1,0:T(8,128)}, u32[]{:S(2)}) copy-start(f32[2,1,256,512]{3,2,1,0:T(8,128)} %param.18) | copy-start | bytes 3145732
  9.6 13.8 %all-to-all-start = ((bf16[2,8,256]{2,0,1:T(2,128)(2,1)}), bf16[2,8,256]{2,0,1:T(2,128)(2,1)S(1)}, u32[]{:S(2)}, u32[]{:S(2)}) async-start(bf16[2,8,256]{2,0,1:T(2,128)(2,1)} %bitcast), calls=%async_computation | async-start | bytes 16384 | tf_op jit(solution)/shard_map/all_to_all | solution.py:49
  16.9 77.5 %all-reduce.3.cloned.1.call-start = ((), (), s32[]{:S(2)}) async-start(), calls=%async_computation.6 | async-start | bytes 163840
  28.1 0.7 copy-start.12
  95.2 0.7 copy-start.10
  96.7 12.5 %copy-start.5 = (bf16[512,256]{1,0:T(8,128)(2,1)S(1)}, bf16[512,256]{1,0:T(8,128)(2,1)}, u32[]{:S(2)}) copy-start(bf16[512,256]{1,0:T(8,128)(2,1)} %param.26) | copy-start | bytes 786436
  98.3 10.9 %all-to-all-start.1 = ((bf16[8,2,512]{2,1,0:T(2,128)(2,1)}), bf16[8,2,512]{2,1,0:T(2,128)(2,1)S(1)}, u32[]{:S(2)}, u32[]{:S(2)}) async-start(bf16[8,2,512]{2,1,0:T(2,128)(2,1)} %stack.2), calls=%async_computation.1 | async-start | bytes 32768 | tf_op jit(solution)/shard_map/all_to_all | solution.py:80
  109.4 4.7 %copy-start.1 = (bf16[8,2048]{1,0:T(8,128)(2,1)S(1)}, bf16[8,2048]{1,0:T(8,128)(2,1)}, u32[]{:S(2)}) copy-start(bf16[8,2048]{1,0:T(8,128)(2,1)} %param.29) | copy-start | bytes 98308
  110.0 9.8 %all-to-all-start.2 = ((bf16[8,2,256]{2,1,0:T(2,128)(2,1)}), bf16[8,2,256]{2,1,0:T(2,128)(2,1)S(1)}, u32[]{:S(2)}, u32[]{:S(2)}) async-start(bf16[8,2,256]{2,1,0:T(2,128)(2,1)} %all_to_all.39), calls=%async_computation.2 | async-start | bytes 16384 | tf_op jit(solution)/shard_map/all_to_all | solution.py:85
  113.4 61.9 %reduce-scatter.2.cloned.1.call-start = ((), (), s32[]{:S(2)}) async-start(), calls=%async_computation.5 | async-start | bytes 81920 | tf_op jit(solution)/shard_map/reduce_scatter | solution.py:121
  113.4 0.7 copy-start.9
  114.1 42.7 %copy-start.4 = (bf16[1,2048,128]{2,1,0:T(8,128)(2,1)S(1)}, bf16[1,2048,128]{2,1,0:T(8,128)(2,1)}, u32[]{:S(2)}) copy-start(bf16[1,2048,128]{2,1,0:T(8,128)(2,1)} %param.31) | copy-start | bytes 1572868
  119.8 5.9 %copy-start.7 = (bf16[2,2048]{1,0:T(2,128)(2,1)S(1)}, bf16[2,2048]{1,0:T(2,128)(2,1)}, u32[]{:S(2)}) copy-start(bf16[2,2048]{1,0:T(2,128)(2,1)} %param.17) | copy-start | bytes 24580
  125.7 31.3 %copy-start.3 = (bf16[1,2048,128]{2,1,0:T(8,128)(2,1)S(1)}, bf16[1,2048,128]{2,1,0:T(8,128)(2,1)}, u32[]{:S(2)}) copy-start(bf16[1,2048,128]{2,1,0:T(8,128)(2,1)} %param.32) | copy-start | bytes 1572868
  158.0 0.7 copy-start.11
  176.8 12.1 %all-to-all-start.3 = ((bf16[8,2,512]{2,1,0:T(2,128)(2,1)}), bf16[8,2,512]{2,1,0:T(2,128)(2,1)S(1)}, u32[]{:S(2)}, u32[]{:S(2)}) async-start(bf16[8,2,512]{2,1,0:T(2,128)(2,1)} %convert_element_type.128), calls=%async_computation.4 | async-start | bytes 32768 | tf_op jit(solution)/shard_map/all_to_all | solution.py:129
Sparse Core Ops, SparseCore 0:
  27.6 66.7 all-reduce.2
  158.1 17.0 reduce-scatter.1
